TPU v7x, 32 devices: a whole 2x2x4 slice. The times are simulated.
32 devices in a mesh: grp: 2 (over y), sp: 2 (over x), tp: 4 (over z), dp: 2 (over core).
Axes of the slice: x: 2, y: 2, z: 4, core: 2. Of those that a mesh axis runs over, the one named last changes fastest.
Arguments:
- latent: bfloat16 [4, 768, 2048], P(('grp', 'dp'), ('sp', 'tp')), parts along dimension 0, may hold values from -6 to 6
- cond: bfloat16 [4, 2048], P(('grp', 'dp')), parts along dimension 0, may hold values from -6 to 6
- context: bfloat16 [4, 256, 2048], P(('grp', 'dp'), 'sp'), parts along dimension 0, may hold values from -6 to 6
- cond_ctx: bfloat16 [2048], replicated, may hold values from -8 to 8
- w_shift: bfloat16 [2048, 2048], P('sp', 'tp'), may hold values from -0.125 to 0.125
- w_scale: bfloat16 [2048, 2048], P('sp', 'tp'), may hold values from -0.125 to 0.125
- w_gate: bfloat16 [2048, 2048], P('sp', 'tp'), may hold values from -0.125 to 0.125
- norm_gain: float32 [2048], replicated, may hold values from 0.1 to 1.9
- w_query: bfloat16 [2048, 1024], P(None, 'tp'), may hold values from -0.125 to 0.125
- w_key: bfloat16 [2048, 512], P(None, 'tp'), may hold values from -0.125 to 0.125
- w_value: bfloat16 [2048, 512], P(None, 'tp'), may hold values from -0.125 to 0.125
- query_gain: float32 [128], replicated, may hold values from 0.6 to 16
- key_gain: float32 [128], replicated, may hold values from 0.6 to 16
- ctx_lift: float32 [8], P('tp'), may hold values from -2 to 0.5
- out_gain: float32 [1024], replicated, may hold values from 0.1 to 1.9
- w_out: bfloat16 [1024, 2048], replicated, may hold values from -0.1875 to 0.1875
Outputs:
- result: bfloat16 [4, 768, 2048], P(('grp', 'dp'), ('sp', 'tp')), parts along dimension 0
There are 2 independent parts, one for each index of `grp`. A program takes and returns all parts, laid end to end along the dimension named above; an argument that names none is the same for every part. Nothing has to cross between parts.
All inputs are finite; a program needn't handle non-finite values.
Results may differ from a plain program's by a relative error of at most 0.023.
The roundings to bfloat16 on the way count: a program that leaves them out, or rounds other values in their place, can miss the bound.
Values may be sent and summed in bfloat16 or wider, within the bound.
A program may use at most 64 MiB of HBM per device.

v0:
```python
import functools
import math

import jax
import jax.numpy as jnp
import numpy as np
from jax import lax
from jax.experimental import pallas as pl
from jax.experimental.pallas import tpu as pltpu
from jax.sharding import PartitionSpec as P

HEAD_DIM = 128
GRID_WIDTH = 64
EPSILON = 1e-06
MESH = pl.DeviceIdType.MESH
F32 = jnp.float32
BF16 = jnp.bfloat16


def position_tables(count):
    freqs = HEAD_DIM // 4
    places = np.arange(count)
    inverse = 10000.0 ** (-np.arange(freqs) / freqs)
    rows = (places // GRID_WIDTH)[:, None] * inverse
    cols = (places % GRID_WIDTH)[:, None] * inverse
    angles = np.concatenate([rows, rows, cols, cols], 1)
    signs = np.concatenate([-np.ones(freqs), np.ones(freqs)] * 2)
    return np.stack([np.cos(angles), np.sin(angles) * signs]).astype(np.float32)


def kernel(n_sp, n_tp, *refs):
    (latent_h, cond_h, context_h, cond_ctx_h, ws_h, wc_h, wg_h, gain_h, wq_h, wk_h, wv_h,
     qgain_h, kgain_h, lift_h, ogain_h, wout_h, table_h, out_ref,
     x_all, cond_v, cond_ctx_v, ctx_v, wmod, gain_v, wqkv, qgain_v, kgain_v, lift_v, ogain_v,
     wout_v, table_v, mod_send, mod_recv, kv_lat, kv_ctx, q_buf, att_send, att_recv,
     load_sem, ctx_flat, r_send, r_recv, l_send, l_recv, m_send, m_recv,
     k_send, k_recv, a_send, a_recv) = refs
    sp = lax.axis_index("sp")
    tp = lax.axis_index("tp")
    rows, width = x_all.shape[1:]
    ctx_rows = ctx_v.shape[0]
    in_rows, mod_cols = wmod.shape[1:]
    q_cols = wq_h.shape[1]
    group = q_cols // HEAD_DIM
    half = rows // 2
    small = half - half // 3
    spans = ((0, small), (small, half - small), (half, small), (half + small, half - small))

    loads = {
        "latent": (latent_h.at[0], x_all.at[tp]),
        "cond": (cond_h, cond_v),
        "cond_ctx": (cond_ctx_h, cond_ctx_v),
        "ws": (ws_h, wmod.at[0]),
        "wc": (wc_h, wmod.at[1]),
        "wg": (wg_h, wmod.at[2]),
        "ctx": (context_h.at[0], ctx_v),
        "gain": (gain_h, gain_v),
        "wk": (wk_h, wqkv.at[:, pl.ds(q_cols, HEAD_DIM)]),
        "wv": (wv_h, wqkv.at[:, pl.ds(q_cols + HEAD_DIM, HEAD_DIM)]),
        "wq": (wq_h, wqkv.at[:, pl.ds(0, q_cols)]),
        "kgain": (kgain_h, kgain_v),
        "qgain": (qgain_h, qgain_v),
        "table": (
            table_h.at[:, pl.ds(pl.multiple_of(sp * (n_tp * rows), n_tp * rows), n_tp * rows)],
            table_v,
        ),
        "lift": (lift_h, lift_v),
        "ogain": (ogain_h, ogain_v),
        "wout": (wout_h, wout_v),
    }
    copies = {}
    for place, (name, (src, dst)) in enumerate(loads.items()):
        copies[name] = pltpu.make_async_copy(src, dst, load_sem.at[place])
        copies[name].start()

    def ready(*names):
        for name in names:
            copies[name].wait()

    def peer(ds, dt):
        return {"sp": lax.rem(sp + ds, n_sp), "tp": lax.rem(tp + dt, n_tp)}

    others = [(ds, dt) for ds in range(n_sp) for dt in range(n_tp) if (ds, dt) != (0, 0)]
    barrier = pltpu.get_barrier_semaphore()
    for ds, dt in others:
        pl.semaphore_signal(barrier, inc=1, device_id=peer(ds, dt), device_id_type=MESH)
    pl.semaphore_wait(barrier, len(others))

    sent = []

    def remote(src, dst, send_sem, recv_sem, target):
        return pltpu.make_async_remote_copy(
            src_ref=src, dst_ref=dst, send_sem=send_sem, recv_sem=recv_sem,
            device_id=target, device_id_type=MESH,
        )

    def send(copy):
        copy.start()
        sent.append(copy)

    def ring_right(step, part):
        block = lax.rem(tp - (step - 1) + n_tp, n_tp)
        piece = x_all.at[block, pl.ds(*spans[part])]
        return remote(piece, piece, r_send.at[step - 1, part], r_recv.at[step - 1, part], peer(0, 1))

    def ring_left(step, part):
        block = lax.rem(tp + (step - 1), n_tp)
        piece = x_all.at[block, pl.ds(*spans[part])]
        return remote(
            piece, piece, l_send.at[step - 1, part], l_recv.at[step - 1, part], peer(0, n_tp - 1)
        )

    def right_parts(step):
        return (0, 1) if 2 * step == n_tp else (0, 1, 2, 3)

    def left_parts(step):
        return (2, 3) if 2 * step == n_tp else (2, 3, 0, 1)

    steps = n_tp // 2
    ready("latent")
    if steps:
        for part in range(2):
            send(ring_right(1, right_parts(1)[part]))
            send(ring_left(1, left_parts(1)[part]))

    ready("cond", "cond_ctx")
    begin = pl.multiple_of(sp * in_rows, in_rows)
    own = cond_v[:, pl.ds(begin, in_rows)].astype(F32)
    ctx_flat[...] = cond_ctx_v[...].astype(F32).reshape(1, width)
    own_ctx = ctx_flat[:, pl.ds(begin, in_rows)]
    own = own * jax.nn.sigmoid(own)
    own_ctx = own_ctx * jax.nn.sigmoid(own_ctx)
    row_id = lax.broadcasted_iota(jnp.int32, (8, in_rows), 0)
    partial_mod = jnp.zeros((8, mod_cols), F32)
    for place, name in enumerate(("ws", "wc", "wg")):
        stacked = jnp.where(row_id == 2 * place, own, 0.0)
        stacked = jnp.where(row_id == 2 * place + 1, own_ctx, stacked).astype(BF16)
        ready(name)
        partial_mod += jnp.dot(stacked, wmod[place], preferred_element_type=F32)
    mod_send[...] = partial_mod
    mod_recv[sp, tp] = partial_mod

    mods = {}
    for ds, dt in sorted(others, key=lambda pair: -min(pair[1], n_tp - pair[1])):
        place = ds * n_tp + dt
        mods[place] = remote(
            mod_send, mod_recv.at[sp, tp], m_send.at[place], m_recv.at[place], peer(ds, dt)
        )
        send(mods[place])
    if steps:
        for part in right_parts(1)[2:]:
            send(ring_right(1, part))
        for part in left_parts(1)[2:]:
            send(ring_left(1, part))

    waited = set()

    def arrive_right(step, part):
        if ("r", step, part) not in waited:
            waited.add(("r", step, part))
            ring_right(step, part).wait_recv()

    def arrive_left(step, part):
        if ("l", step, part) not in waited:
            waited.add(("l", step, part))
            ring_left(step, part).wait_recv()

    for step in range(1, steps):
        for part_r, part_l in zip(right_parts(step), left_parts(step)):
            if part_r in right_parts(step + 1):
                arrive_right(step, part_r)
                send(ring_right(step + 1, part_r))
            if part_l in left_parts(step + 1):
                arrive_left(step, part_l)
                send(ring_left(step + 1, part_l))

    for copy in mods.values():
        copy.wait_recv()
    total_mod = mod_recv[0]
    for place in range(1, n_sp):
        total_mod = total_mod + mod_recv[place]
    modulation = jnp.concatenate([total_mod[place] for place in range(n_tp)], 1)
    ready("gain")
    gain_row = gain_v[...]
    shift = modulation[0:1]
    weight = gain_row * (1.0 + modulation[2:3])
    ctx_shift = modulation[1:2]
    ctx_weight = gain_row * (1.0 + modulation[3:4])
    gate = modulation[4:5]

    def pre_norm(data, weight_row, shift_row):
        floats = data.astype(F32)
        inverse = lax.rsqrt(jnp.mean(floats * floats, -1, keepdims=True) + EPSILON)
        return (floats * inverse * weight_row + shift_row).astype(BF16)

    def head_norm(projected, gain_vector):
        floats = projected.astype(BF16).astype(F32)
        return floats * lax.rsqrt(jnp.mean(floats * floats, -1, keepdims=True) + EPSILON) * gain_vector

    quarter = HEAD_DIM // 4
    lane = lax.broadcasted_iota(jnp.int32, (1, HEAD_DIM), 1)
    first = lax.rem(lane, 2 * quarter) < quarter

    def rotate(vectors, cosine, sine):
        swapped = jnp.where(
            first, pltpu.roll(vectors, HEAD_DIM - quarter, 1), pltpu.roll(vectors, quarter, 1)
        )
        return vectors * cosine + swapped * sine

    shared = []

    def share(buffer, place):
        for ds in range(1, n_sp):
            copy = remote(
                buffer, buffer, k_send.at[place, ds], k_recv.at[place, ds],
                {"sp": lax.rem(sp + ds, n_sp)},
            )
            send(copy)
            shared.append(copy)

    ready("ctx", "wk", "wv", "kgain")
    kgain = kgain_v[...]
    ctx_kv = jnp.dot(
        pre_norm(ctx_v[...], ctx_weight, ctx_shift), wqkv[:, q_cols:], preferred_element_type=F32
    )
    kv_ctx[sp, :, :HEAD_DIM] = head_norm(ctx_kv[:, :HEAD_DIM], kgain).astype(BF16)
    kv_ctx[sp, :, HEAD_DIM:] = ctx_kv[:, HEAD_DIM:].astype(BF16)
    share(kv_ctx.at[sp], n_tp)

    ready("wq", "qgain", "table")
    qgain = qgain_v[...]

    def project(block, place, parts=((0, rows),), slot=0):
        count = sum(size for _, size in parts)
        normed = pre_norm(
            jnp.concatenate([x_all[block, pl.ds(*part)] for part in parts], 0), weight, shift
        )
        out = jnp.dot(normed, wqkv[...], preferred_element_type=F32)

        def places(which):
            return jnp.concatenate(
                [
                    table_v[which, pl.ds(pl.multiple_of(block * rows + start, 8), size)]
                    for start, size in parts
                ],
                0,
            )

        cosine, sine = places(0), places(1)
        key = rotate(head_norm(out[:, q_cols : q_cols + HEAD_DIM], kgain), cosine, sine)
        kv_lat[sp, block, pl.ds(slot, count), :HEAD_DIM] = key.astype(BF16)
        kv_lat[sp, block, pl.ds(slot, count), HEAD_DIM:] = out[:, q_cols + HEAD_DIM :].astype(BF16)
        share(kv_lat.at[sp, block, pl.ds(slot, count)], place)
        for head in range(group):
            query = head_norm(out[:, head * HEAD_DIM : (head + 1) * HEAD_DIM], qgain)
            query = rotate(query, cosine, sine).astype(BF16)
            begin = 0
            for start, size in parts:
                q_buf[block, pl.ds(head * rows + start, size)] = query[begin : begin + size]
                begin += size

    project(tp, 0)
    for step in range(1, steps):
        for part in right_parts(step):
            arrive_right(step, part)
        project(lax.rem(tp - step + n_tp, n_tp), n_tp - step)
        for part in left_parts(step):
            arrive_left(step, part)
        project(lax.rem(tp + step, n_tp), step)

    for copy in shared:
        copy.wait_recv()
    near_shared = len(shared)
    ready("lift")
    factor = HEAD_DIM ** (-0.5)
    ratio = math.log(n_tp * rows / ctx_rows)
    lifts = jnp.concatenate(
        [jnp.broadcast_to(lift_v[0:1, head : head + 1] + ratio, (rows, 1)) for head in range(group)], 0
    )
    contract = (((1,), (1,)), ((), ()))
    far = steps

    def block_at(offset):
        return lax.rem(tp + offset, n_tp)

    def latent_part(offsets, channels):
        return jnp.concatenate(
            [
                kv_lat[place, block_at(offset), :, channels]
                for place in range(n_sp)
                for offset in offsets
            ],
            0,
        )

    key_part = slice(0, HEAD_DIM)
    value_part = slice(HEAD_DIM, 2 * HEAD_DIM)

    def scores_of(query, keys):
        return lax.dot_general(query, keys, contract, preferred_element_type=F32) * factor

    near = [offset for offset in range(n_tp) if offset != far]
    ctx_count = n_sp * ctx_rows

    def attend_near(offset):
        query = q_buf[block_at(offset)]
        scores = scores_of(query, latent_part(near, key_part))
        ctx_scores = scores_of(query, kv_ctx[:, :, key_part].reshape(ctx_count, HEAD_DIM)) + lifts
        highest = jnp.maximum(
            jnp.max(scores, -1, keepdims=True), jnp.max(ctx_scores, -1, keepdims=True)
        )
        weights = jnp.exp(scores - highest)
        ctx_weights = jnp.exp(ctx_scores - highest)
        total = jnp.sum(weights, -1, keepdims=True) + jnp.sum(ctx_weights, -1, keepdims=True)
        summed = jnp.dot(
            weights.astype(BF16), latent_part(near, value_part), preferred_element_type=F32
        ) + jnp.dot(
            ctx_weights.astype(BF16),
            kv_ctx[:, :, value_part].reshape(ctx_count, HEAD_DIM),
            preferred_element_type=F32,
        )
        return highest, total, summed

    def attend_far(offset, carried):
        highest, total, summed = carried
        scores = scores_of(q_buf[block_at(offset)], latent_part([far], key_part))
        topmost = jnp.maximum(highest, jnp.max(scores, -1, keepdims=True))
        keep = jnp.exp(highest - topmost)
        weights = jnp.exp(scores - topmost)
        total = total * keep + jnp.sum(weights, -1, keepdims=True)
        summed = summed * keep + jnp.dot(
            weights.astype(BF16), latent_part([far], value_part), preferred_element_type=F32
        )
        result = (summed / total).astype(BF16)
        return [result[head * rows : (head + 1) * rows] for head in range(group)]

    carried = {offset: attend_near(offset) for offset in near}
    for piece in range(2):
        arrive_right(steps, piece)
        arrive_left(steps, 2 + piece)
        parts = (spans[piece], spans[2 + piece])
        project(
            block_at(far), far if piece == 0 else n_tp + 1, parts, 0 if piece == 0 else 2 * small
        )
    carried[far] = attend_near(far)
    for copy in shared[near_shared:]:
        copy.wait_recv()

    returned = []
    for dt in sorted(range(1, n_tp), key=lambda d: -min(d, n_tp - d)):
        for head, piece in enumerate(attend_far(dt, carried[dt])):
            att_send[dt, :, head * HEAD_DIM : (head + 1) * HEAD_DIM] = piece
        copy = remote(
            att_send.at[dt], att_recv.at[tp], a_send.at[dt], a_recv.at[dt], {"tp": block_at(dt)}
        )
        send(copy)
        returned.append(copy)
    for head, piece in enumerate(attend_far(0, carried[0])):
        att_recv[tp, :, head * HEAD_DIM : (head + 1) * HEAD_DIM] = piece
    ready("ogain", "wout")
    for copy in returned:
        copy.wait_recv()

    tokens = jnp.concatenate([att_recv[place] for place in range(n_tp)], 1).astype(F32)
    inverse = lax.rsqrt(jnp.mean(tokens * tokens, -1, keepdims=True) + EPSILON)
    att_normed = (tokens * inverse * ogain_v[...]).astype(BF16)
    wide = width // 2
    for place in range(2):
        columns = slice(place * wide, (place + 1) * wide)
        mixture = jnp.dot(att_normed, wout_v[:, columns], preferred_element_type=F32)
        out_ref[0, :, columns] = (
            x_all[tp, :, columns].astype(F32) + gate[:, columns] * mixture
        ).astype(BF16)
    for copy in sent:
        copy.wait_send()


def solution(mesh):
    n_sp, n_tp = mesh.shape["sp"], mesh.shape["tp"]

    def on_device(latent, cond, context, cond_ctx, w_shift, w_scale, w_gate, norm_gain, w_query,
                  w_key, w_value, query_gain, key_gain, ctx_lift, out_gain, w_out):
        rows, width = latent.shape[1:]
        ctx_rows = context.shape[1]
        in_rows, mod_cols = w_shift.shape
        q_cols, k_cols = w_query.shape[1], w_key.shape[1]
        assert k_cols == HEAD_DIM and rows % 96 == 0 and n_tp % 2 == 0
        group = q_cols // HEAD_DIM
        inner = w_out.shape[0]
        table = jnp.asarray(position_tables(n_sp * n_tp * rows))
        steps = max(n_tp // 2, 1)
        operands = (
            latent, cond, context, cond_ctx, w_shift, w_scale, w_gate, norm_gain[None],
            w_query, w_key, w_value, query_gain[None], key_gain[None], ctx_lift[None],
            out_gain[None], w_out, table,
        )
        dma = pltpu.SemaphoreType.DMA
        return pl.pallas_call(
            functools.partial(kernel, n_sp, n_tp),
            out_shape=pltpu.VMEM(latent.shape, BF16),
            in_specs=[pl.BlockSpec(memory_space=pl.ANY)] * len(operands),
            out_specs=pl.BlockSpec(memory_space=pltpu.VMEM),
            scratch_shapes=[
                pltpu.VMEM((n_tp, rows, width), BF16),
                pltpu.VMEM((1, width), BF16),
                pltpu.VMEM((width,), BF16),
                pltpu.VMEM((ctx_rows, width), BF16),
                pltpu.VMEM((3, in_rows, mod_cols), BF16),
                pltpu.VMEM((1, width), F32),
                pltpu.VMEM((width, q_cols + 2 * HEAD_DIM), BF16),
                pltpu.VMEM((1, HEAD_DIM), F32),
                pltpu.VMEM((1, HEAD_DIM), F32),
                pltpu.VMEM((1, group), F32),
                pltpu.VMEM((1, inner), F32),
                pltpu.VMEM((inner, width), BF16),
                pltpu.VMEM((2, n_tp * rows, HEAD_DIM), F32),
                pltpu.VMEM((8, mod_cols), F32),
                pltpu.VMEM((n_sp, n_tp, 8, mod_cols), F32),
                pltpu.VMEM((n_sp, n_tp, rows, 2 * HEAD_DIM), BF16),
                pltpu.VMEM((n_sp, ctx_rows, 2 * HEAD_DIM), BF16),
                pltpu.VMEM((n_tp, group * rows, HEAD_DIM), BF16),
                pltpu.VMEM((n_tp, rows, q_cols), BF16),
                pltpu.VMEM((n_tp, rows, q_cols), BF16),
                dma((len(operands),)),
                pltpu.VMEM((1, width), F32),
                dma((steps, 4)),
                dma((steps, 4)),
                dma((steps, 4)),
                dma((steps, 4)),
                dma((n_sp * n_tp,)),
                dma((n_sp * n_tp,)),
                dma((n_tp + 2, n_sp)),
                dma((n_tp + 2, n_sp)),
                dma((n_tp,)),
                dma((n_tp,)),
            ],
            compiler_params=pltpu.CompilerParams(
                collective_id=0, has_side_effects=True, vmem_limit_bytes=60 * 2**20
            ),
        )(*operands)

    in_specs = (
        P(("grp", "dp"), ("sp", "tp"), None),
        P(("grp", "dp"), None),
        P(("grp", "dp"), "sp", None),
        P(),
        P("sp", "tp"),
        P("sp", "tp"),
        P("sp", "tp"),
        P(),
        P(None, "tp"),
        P(None, "tp"),
        P(None, "tp"),
        P(),
        P(),
        P("tp"),
        P(),
        P(),
    )
    out_specs = P(("grp", "dp"), ("sp", "tp"), None)
    return jax.shard_map(
        on_device, mesh=mesh, in_specs=in_specs, out_specs=out_specs, check_vma=False
    )
```

profile of v0, /device:TPU:0, one launch (start us, length us, event | category | flops | bytes accessed | tf_op | source)
XLA Modules:
  0.0 46.4 jit_solution(5931755044944492710)
XLA Ops:
  0.0 45.6 %shard_map.163 = bf16[1,96,2048]{2,1,0:T(8,128)(2,1)S(1)} custom-call(bf16[1,96,2048]{2,1,0:T(8,128)(2,1)} %refs_0_.1, bf16[1,2048]{1,0:T(2,128)(2,1)} %refs_1_.1, bf16[1,128,2048]{2,1,0:T(8,128)(2,1)} %refs_2_.1, bf16[2048]{0:T(1024)(128)(2,1)} %refs_3_.1, bf16[1024,512]{1,0:T(8,128)(2,1)} %refs_4_.1, bf16[1024,512]{1,0:T(8,128)(2,1)} %refs_5_.1, ...), custom_call_target="tpu_custom_call" | custom-call | tf_op jit(solution)/shard_map/pallas_call | solution.py:398
  45.6 0.7 %copy.19 = bf16[1,96,2048]{2,1,0:T(8,128)(2,1)} copy(bf16[1,96,2048]{2,1,0:T(8,128)(2,1)S(1)} %shard_map.163) | data formatting | bytes 786432
where the time goes:
time: 46.5 us; the launch traced here: 46.4 us
  Pallas kernels  45.6 us (98%)
  local copies, waits for them, and re-layouts  0.75 us (2%)
    pallas_call x1, Pallas kernels, on_device(): pl.pallas_call(functools.partial(kernel, n_sp, n_tp), out_shape=pltpu.VME...  45.6 us

commit v1 on v0

--- a/solution.py
+++ b/solution.py
@@ -28,7 +28,7 @@
     return np.stack([np.cos(angles), np.sin(angles) * signs]).astype(np.float32)
 
 
-def kernel(n_sp, n_tp, *refs):
+def ring_kernel(n_sp, n_tp, *refs):
     (latent_h, cond_h, context_h, cond_ctx_h, ws_h, wc_h, wg_h, gain_h, wq_h, wk_h, wv_h,
      qgain_h, kgain_h, lift_h, ogain_h, wout_h, table_h, out_ref,
      x_all, cond_v, cond_ctx_v, ctx_v, wmod, gain_v, wqkv, qgain_v, kgain_v, lift_v, ogain_v,
@@ -375,8 +375,640 @@
         copy.wait_send()
 
 
+PARTS = 6
+PIECES = ((0, 4), (4, 2))
+SHARD_PIECES = 4
+
+
+def line_kernel(*refs):
+    (latent_h, cond_h, context_h, cond_ctx_h, ws_h, wc_h, wg_h, gain_h, wq_h, wk_h, wv_h,
+     qgain_h, kgain_h, lift_h, ogain_h, wout_h, table_h, out_ref,
+     x_all, cond_v, cond_ctx_v, ctx_v, wmod, gain_v, wqkv, wext, wshard, qgain_v, kgain_v,
+     lift_v, ogain_v, wout_v, table_v, mod_send, mod_near, mod_sum, mod_all, kv_lat, kv_ctx,
+     q_buf, q_ship, kv_ship, att_send, att_recv, ctx_flat,
+     load_sem, token, near_s, in_s, x_recv, mx_s, mx_r, mz_s, mz_r, k_s, k_r, a_s, a_r,
+     wz_s, wz_r, wx_s, wx_r, wy_s, wy_r, wc_s, wc_r, qs_s, qs_r, kvs_s, kvs_r) = refs
+    n_tp = x_all.shape[0]
+    n_sp = kv_lat.shape[0]
+    sp = lax.axis_index("sp")
+    tp = lax.axis_index("tp")
+    grp = lax.axis_index("grp")
+    dp = lax.axis_index("dp")
+    rows, width = x_all.shape[1:]
+    ctx_rows = ctx_v.shape[0]
+    in_rows, mod_cols = wmod.shape[1:]
+    q_cols = wq_h.shape[1]
+    group = q_cols // HEAD_DIM
+    part_rows = rows // PARTS
+    shard_rows = wshard.shape[0]
+    piece_rows = shard_rows // SHARD_PIECES
+
+    half = lax.div(tp, 2)
+    pair = tp + 1 - 2 * lax.rem(tp, 2)
+    cross = n_tp // 2 - half
+    hub = jnp.logical_or(tp == n_tp // 2 - 1, tp == n_tp // 2)
+    edge = jnp.logical_not(hub)
+    is_hub = hub.astype(jnp.int32)
+    far_end = (n_tp - 1) * (1 - half)
+    order = (
+        tp,
+        is_hub * cross + (1 - is_hub) * pair,
+        is_hub * pair + (1 - is_hub) * cross,
+        far_end,
+    )
+
+    shard_begin = pl.multiple_of(((sp * 2 + grp) * 2 + dp) * shard_rows, shard_rows)
+    loads = {
+        "latent": (latent_h.at[0], x_all.at[0]),
+        "sq": (wq_h.at[pl.ds(shard_begin, shard_rows)], wshard.at[:, pl.ds(0, q_cols)]),
+        "sk": (wk_h.at[pl.ds(shard_begin, shard_rows)], wshard.at[:, pl.ds(q_cols, HEAD_DIM)]),
+        "sv": (
+            wv_h.at[pl.ds(shard_begin, shard_rows)],
+            wshard.at[:, pl.ds(q_cols + HEAD_DIM, HEAD_DIM)],
+        ),
+        "cond": (cond_h, cond_v),
+        "cond_ctx": (cond_ctx_h, cond_ctx_v),
+        "ws": (ws_h, wmod.at[0]),
+        "wc": (wc_h, wmod.at[1]),
+        "wg": (wg_h, wmod.at[2]),
+        "ctx": (context_h.at[0], ctx_v),
+        "gain": (gain_h, gain_v),
+        "wk": (wk_h, wqkv.at[:, pl.ds(q_cols, HEAD_DIM)]),
+        "wv": (wv_h, wqkv.at[:, pl.ds(q_cols + HEAD_DIM, HEAD_DIM)]),
+        "wq": (wq_h, wqkv.at[:, pl.ds(0, q_cols)]),
+        "kgain": (kgain_h, kgain_v),
+        "qgain": (qgain_h, qgain_v),
+        "table": (
+            table_h.at[:, pl.ds(pl.multiple_of(sp * (n_tp * rows), n_tp * rows), n_tp * rows)],
+            table_v,
+        ),
+        "lift": (lift_h, lift_v),
+        "ogain": (ogain_h, ogain_v),
+        "wout": (wout_h, wout_v),
+    }
+    copies = {}
+    for place, (name, (src, dst)) in enumerate(loads.items()):
+        copies[name] = pltpu.make_async_copy(src, dst, load_sem.at[place])
+        copies[name].start()
+
+    def ready(*names):
+        for name in names:
+            copies[name].wait()
+
+    to_x = {"sp": 1 - sp}
+    to_y = {"grp": 1 - grp}
+    to_core = {"dp": 1 - dp}
+    to_pair = {"tp": pair}
+    to_cross = {"tp": cross}
+
+    barrier = pltpu.get_barrier_semaphore()
+    for target in (to_x, to_y, to_core, to_pair):
+        pl.semaphore_signal(barrier, inc=1, device_id=target, device_id_type=MESH)
+
+    @pl.when(hub)
+    def _():
+        pl.semaphore_signal(barrier, inc=1, device_id=to_cross, device_id_type=MESH)
+
+    ready("latent", "sq", "sk", "sv")
+    pl.semaphore_wait(barrier, 4 + is_hub)
+
+    sent = []
+    hub_sent = []
+    edge_sent = []
+
+    def remote(src, dst, send_sem, recv_sem, target):
+        return pltpu.make_async_remote_copy(
+            src_ref=src, dst_ref=dst, send_sem=send_sem, recv_sem=recv_sem,
+            device_id=target, device_id_type=MESH,
+        )
+
+    def part_of(slot, part):
+        return x_all.at[slot, pl.ds(part * part_rows, part_rows)]
+
+    def raw(src_slot, dst_slot, part, send_sem, target):
+        return remote(
+            part_of(src_slot, part), part_of(dst_slot, part), send_sem,
+            x_recv.at[dst_slot - 1, part], target,
+        )
+
+    def own_out(part):
+        return raw(0, 1, part, near_s.at[0, part], to_pair)
+
+    def own_up(part):
+        return raw(0, 2, part, near_s.at[0, part], to_pair)
+
+    def own_cross(part):
+        return raw(0, 1, part, in_s.at[0, part], to_cross)
+
+    def pass_cross(part):
+        return raw(2, 3, part, in_s.at[1, part], to_cross)
+
+    def pass_out(part):
+        return raw(1, 2, part, near_s.at[1, part], to_pair)
+
+    def arrive(slot, part):
+        raw(0, slot, part, near_s.at[0, part], to_pair).wait_recv()
+
+    def flip(index, other):
+        return 1 - index if other else index
+
+    def shard_piece(ds, dg, dc, piece):
+        place = (flip(sp, ds) * 2 + flip(grp, dg)) * 2 + flip(dp, dc)
+        return pl.ds(pl.multiple_of(place * shard_rows + piece * piece_rows, piece_rows), piece_rows)
+
+    def w_up(piece):
+        return remote(
+            wshard.at[pl.ds(piece * piece_rows, piece_rows)], wext.at[shard_piece(0, 0, 0, piece)],
+            wz_s.at[piece], wz_r.at[piece], to_pair,
+        )
+
+    def w_move(way, place, ds, dg, piece):
+        send_sem, recv_sem, target = {
+            "x": (wx_s, wx_r, to_x), "y": (wy_s, wy_r, to_y), "core": (wc_s, wc_r, to_core),
+        }[way]
+        block = wext.at[shard_piece(ds, dg, 0, piece)]
+        return remote(block, block, send_sem.at[place], recv_sem.at[place], target)
+
+    def start_all(group_of, store):
+        for make, *given in group_of:
+            make(*given).start()
+            store.append((make, given))
+
+    early = PARTS // 2
+
+    @pl.when(edge)
+    def _():
+        start_all([(w_up, piece) for piece in range(3)], edge_sent)
+
+    @pl.when(hub)
+    def _():
+        for part in range(early):
+            start_all([(own_cross, part), (own_out, part)], hub_sent)
+        pl.semaphore_signal(token, inc=1, device_id=to_cross, device_id_type=MESH)
+
+    ready("cond", "cond_ctx")
+    begin = pl.multiple_of(sp * in_rows, in_rows)
+    own = cond_v[:, pl.ds(begin, in_rows)].astype(F32)
+    ctx_flat[...] = cond_ctx_v[...].astype(F32).reshape(1, width)
+    own_ctx = ctx_flat[:, pl.ds(begin, in_rows)]
+    own = own * jax.nn.sigmoid(own)
+    own_ctx = own_ctx * jax.nn.sigmoid(own_ctx)
+    row_id = lax.broadcasted_iota(jnp.int32, (8, in_rows), 0)
+    partial_mod = jnp.zeros((8, mod_cols), F32)
+    for place, name in enumerate(("ws", "wc", "wg")):
+        stacked = jnp.where(row_id == 2 * place, own, 0.0)
+        stacked = jnp.where(row_id == 2 * place + 1, own_ctx, stacked).astype(BF16)
+        ready(name)
+        partial_mod += jnp.dot(stacked, wmod[place], preferred_element_type=F32)
+    mod_send[...] = partial_mod
+    across = remote(mod_send, mod_near, mx_s, mx_r, to_x)
+    across.start()
+    sent.append(across)
+    across.wait_recv()
+    total_mod = partial_mod + mod_near[...]
+    mod_sum[...] = total_mod
+    mod_all[tp] = total_mod
+
+    pl.semaphore_wait(token, 1)
+
+    @pl.when(hub)
+    def _():
+        pl.semaphore_signal(token, inc=1, device_id=to_pair, device_id_type=MESH)
+
+    mods = []
+    for dt in range(1, n_tp):
+        copy = remote(
+            mod_sum, mod_all.at[tp], mz_s.at[dt], mz_r.at[dt], {"tp": lax.rem(tp + dt, n_tp)}
+        )
+        copy.start()
+        sent.append(copy)
+        mods.append(copy)
+
+    @pl.when(edge)
+    def _():
+        start_all([(w_up, piece) for piece in range(3, SHARD_PIECES)], edge_sent)
+        start_all([(own_up, part) for part in range(PARTS)], edge_sent)
+
+    @pl.when(hub)
+    def _():
+        for part in range(early, PARTS):
+            start_all([(own_cross, part), (own_out, part)], hub_sent)
+        for piece in range(SHARD_PIECES):
+            w_up(piece).wait_recv()
+            start_all(
+                [
+                    (w_move, "x", piece, 0, 0, piece),
+                    (w_move, "y", piece, 0, 0, piece),
+                    (w_move, "core", (0, piece), 0, 0, piece),
+                ],
+                hub_sent,
+            )
+
+    for copy in mods:
+        copy.wait_recv()
+    modulation = jnp.concatenate([mod_all[place] for place in range(n_tp)], 1)
+    ready("gain")
+    gain_row = gain_v[...]
+    shift = modulation[0:1]
+    weight = gain_row * (1.0 + modulation[2:3])
+    ctx_shift = modulation[1:2]
+    ctx_weight = gain_row * (1.0 + modulation[3:4])
+    gate = modulation[4:5]
+
+    def pre_norm(data, weight_row, shift_row):
+        floats = data.astype(F32)
+        inverse = lax.rsqrt(jnp.mean(floats * floats, -1, keepdims=True) + EPSILON)
+        return (floats * inverse * weight_row + shift_row).astype(BF16)
+
+    def head_norm(projected, gain_vector):
+        floats = projected.astype(BF16).astype(F32)
+        return floats * lax.rsqrt(jnp.mean(floats * floats, -1, keepdims=True) + EPSILON) * gain_vector
+
+    quarter = HEAD_DIM // 4
+    lane = lax.broadcasted_iota(jnp.int32, (1, HEAD_DIM), 1)
+    first = lax.rem(lane, 2 * quarter) < quarter
+
+    def rotate(vectors, cosine, sine):
+        swapped = jnp.where(
+            first, pltpu.roll(vectors, HEAD_DIM - quarter, 1), pltpu.roll(vectors, quarter, 1)
+        )
+        return vectors * cosine + swapped * sine
+
+    def share(buffer, place):
+        copy = remote(buffer, buffer, k_s.at[place], k_r.at[place], to_x)
+        copy.start()
+        return copy
+
+    ready("ctx", "wk", "wv", "kgain")
+    kgain = kgain_v[...]
+    ctx_kv = jnp.dot(
+        pre_norm(ctx_v[...], ctx_weight, ctx_shift), wqkv[:, q_cols:], preferred_element_type=F32
+    )
+    kv_ctx[sp, :, :HEAD_DIM] = head_norm(ctx_kv[:, :HEAD_DIM], kgain).astype(BF16)
+    kv_ctx[sp, :, HEAD_DIM:] = ctx_kv[:, HEAD_DIM:].astype(BF16)
+    shared = {"ctx": share(kv_ctx.at[sp], 0)}
+
+    ready("wq", "qgain", "table")
+    qgain = qgain_v[...]
+
+    def finish(out, slot, start, count, q_dst, kv_dst):
+        place = pl.multiple_of(order[slot] * rows + start, 8)
+        cosine = table_v[0, pl.ds(place, count)]
+        sine = table_v[1, pl.ds(place, count)]
+        key = rotate(head_norm(out[:, q_cols : q_cols + HEAD_DIM], kgain), cosine, sine)
+        kv_dst[:, :HEAD_DIM] = key.astype(BF16)
+        kv_dst[:, HEAD_DIM:] = out[:, q_cols + HEAD_DIM :].astype(BF16)
+        for head in range(group):
+            query = head_norm(out[:, head * HEAD_DIM : (head + 1) * HEAD_DIM], qgain)
+            q_dst[head] = rotate(query, cosine, sine).astype(BF16)
+
+    def normed_rows(slot, start, count):
+        return pre_norm(x_all[slot, pl.ds(start, count)], weight, shift)
+
+    def project(normed, slot, start, count):
+        finish(
+            jnp.dot(normed, wqkv[...], preferred_element_type=F32), slot, start, count,
+            q_buf.at[slot, :, pl.ds(start, count)], kv_lat.at[sp, slot, pl.ds(start, count)],
+        )
+
+    project(normed_rows(0, 0, rows), 0, 0, rows)
+    shared[0] = share(kv_lat.at[sp, 0], 1)
+
+    @pl.when(hub)
+    def _():
+        for part in range(PARTS):
+            arrive(1, part)
+            start_all([(pass_out, part)], hub_sent)
+        for piece in range(SHARD_PIECES):
+            w_move("x", piece, 0, 0, piece).wait_recv()
+            w_move("y", piece, 0, 0, piece).wait_recv()
+            start_all(
+                [
+                    (w_move, "core", (1, piece), 1, 0, piece),
+                    (w_move, "core", (2, piece), 0, 1, piece),
+                ],
+                hub_sent,
+            )
+            spare = SHARD_PIECES + piece % 2
+            if piece < SHARD_PIECES // 2:
+                start_all([(w_move, "y", spare, 1, 0, piece)], hub_sent)
+            else:
+                start_all([(w_move, "x", spare, 0, 1, piece)], hub_sent)
+        for part in range(2):
+            arrive(2, part)
+            start_all([(pass_cross, part)], hub_sent)
+
+    @pl.when(edge)
+    def _():
+        for part in range(PARTS):
+            arrive(1, part)
+
+    project(normed_rows(1, 0, rows), 1, 0, rows)
+    shared[1] = share(kv_lat.at[sp, 1], 2)
+
+    @pl.when(hub)
+    def _():
+        for part in range(2, 4):
+            arrive(2, part)
+            start_all([(pass_cross, part)], hub_sent)
+
+    for name in ("ctx", 0, 1):
+        shared[name].wait_recv()
+    ready("lift")
+    factor = HEAD_DIM ** (-0.5)
+    ratio = math.log(n_tp * rows / ctx_rows)
+    contract = (((1,), (1,)), ((), ()))
+    key_part = slice(0, HEAD_DIM)
+    value_part = slice(HEAD_DIM, 2 * HEAD_DIM)
+    ctx_count = n_sp * ctx_rows
+
+    def scores_of(query, keys):
+        return lax.dot_general(query, keys, contract, preferred_element_type=F32) * factor
+
+    def latent_part(slots, channels):
+        return jnp.concatenate(
+            [kv_lat[place, slot, :, channels] for place in range(n_sp) for slot in slots], 0
+        )
+
+    def query_of(slot, start, count):
+        return q_buf[slot, :, pl.ds(start, count)].reshape(group * count, HEAD_DIM)
+
+    def attend_first(slot, start=0, count=rows):
+        query = query_of(slot, start, count)
+        lifts = jnp.concatenate(
+            [
+                jnp.broadcast_to(lift_v[0:1, head : head + 1] + ratio, (count, 1))
+                for head in range(group)
+            ],
+            0,
+        )
+        scores = scores_of(query, latent_part((0, 1), key_part))
+        ctx_scores = scores_of(query, kv_ctx[:, :, key_part].reshape(ctx_count, HEAD_DIM)) + lifts
+        highest = jnp.maximum(
+            jnp.max(scores, -1, keepdims=True), jnp.max(ctx_scores, -1, keepdims=True)
+        )
+        weights = jnp.exp(scores - highest)
+        ctx_weights = jnp.exp(ctx_scores - highest)
+        total = jnp.sum(weights, -1, keepdims=True) + jnp.sum(ctx_weights, -1, keepdims=True)
+        summed = jnp.dot(
+            weights.astype(BF16), latent_part((0, 1), value_part), preferred_element_type=F32
+        ) + jnp.dot(
+            ctx_weights.astype(BF16),
+            kv_ctx[:, :, value_part].reshape(ctx_count, HEAD_DIM),
+            preferred_element_type=F32,
+        )
+        return highest, total, summed
+
+    def attend_more(carried, key_slot, slot, start=0, count=rows):
+        highest, total, summed = carried
+        scores = scores_of(query_of(slot, start, count), latent_part((key_slot,), key_part))
+        topmost = jnp.maximum(highest, jnp.max(scores, -1, keepdims=True))
+        keep = jnp.exp(highest - topmost)
+        weights = jnp.exp(scores - topmost)
+        total = total * keep + jnp.sum(weights, -1, keepdims=True)
+        summed = summed * keep + jnp.dot(
+            weights.astype(BF16), latent_part((key_slot,), value_part), preferred_element_type=F32
+        )
+        return topmost, total, summed
+
+    carried = {0: attend_first(0)}
+
+    @pl.when(hub)
+    def _():
+        for part in range(4, 5):
+            arrive(2, part)
+            start_all([(pass_cross, part)], hub_sent)
+
+    carried[1] = attend_first(1)
+
+    @pl.when(hub)
+    def _():
+        for part in range(5, PARTS):
+            arrive(2, part)
+            start_all([(pass_cross, part)], hub_sent)
+        for piece in range(SHARD_PIECES):
+            spare = SHARD_PIECES + piece % 2
+            if piece < SHARD_PIECES // 2:
+                w_move("y", spare, 1, 0, piece).wait_recv()
+            else:
+                w_move("x", spare, 0, 1, piece).wait_recv()
+            start_all([(w_move, "core", (3, piece), 1, 1, piece)], hub_sent)
+
+    @pl.when(edge)
+    def _():
+        for part in range(PARTS):
+            arrive(2, part)
+
+    project(normed_rows(2, 0, rows), 2, 0, rows)
+    shared[2] = share(kv_lat.at[sp, 2], 3)
+    carried[2] = attend_first(2)
+
+    far_spans = [(begin * part_rows, count * part_rows) for begin, count in PIECES]
+
+    def ship_query(piece):
+        span = pl.ds(*far_spans[piece])
+        return remote(
+            q_ship.at[:, span], q_buf.at[3, :, span], qs_s.at[piece], qs_r.at[piece], to_pair
+        )
+
+    def ship_keys(piece, place):
+        span = pl.ds(*far_spans[piece])
+        target = {"sp": flip(sp, place), "tp": pair}
+        return remote(
+            kv_ship.at[span], kv_lat.at[sp, 3, span], kvs_s.at[piece, place],
+            kvs_r.at[piece, place], target,
+        )
+
+    def far_share(piece):
+        block = kv_lat.at[sp, 3, pl.ds(*far_spans[piece])]
+        return remote(block, block, k_s.at[4 + piece], k_r.at[4 + piece], to_x)
+
+    def far_piece(piece):
+        start, count = far_spans[piece]
+        begin, parts = PIECES[piece]
+
+        @pl.when(hub)
+        def _():
+            for part in range(begin, begin + parts):
+                arrive(3, part)
+            if piece == 0:
+                for shard in range(4):
+                    for step in range(SHARD_PIECES):
+                        w_move("core", (shard, step), 0, 0, step).wait_recv()
+            normed = normed_rows(3, start, count)
+            finish(
+                jnp.dot(normed, wext[...], preferred_element_type=F32), 3, start, count,
+                q_ship.at[:, pl.ds(start, count)], kv_ship.at[pl.ds(start, count)],
+            )
+            start_all(
+                [(ship_keys, piece, 1), (ship_keys, piece, 0), (ship_query, piece)], hub_sent
+            )
+            project(normed, 3, start, count)
+            start_all([(far_share, piece)], hub_sent)
+
+    def far_wait(piece):
+        @pl.when(hub)
+        def _():
+            far_share(piece).wait_recv()
+
+        @pl.when(edge)
+        def _():
+            for place in range(n_sp):
+                ship_keys(piece, place).wait_recv()
+
+    def far_query_wait(piece):
+        @pl.when(edge)
+        def _():
+            ship_query(piece).wait_recv()
+
+    far_piece(0)
+    shared[2].wait_recv()
+    for slot in range(3):
+        carried[slot] = attend_more(carried[slot], 2, slot)
+    far_query_wait(0)
+    far_carried = [attend_more(attend_first(3, *far_spans[0]), 2, 3, *far_spans[0])]
+    far_piece(1)
+    far_query_wait(1)
+    far_carried.append(attend_more(attend_first(3, *far_spans[1]), 2, 3, *far_spans[1]))
+    far_wait(0)
+    far_wait(1)
+
+    def ready_rows(carried_part, slot, start=0, count=rows):
+        _, total, summed = attend_more(carried_part, 3, slot, start, count)
+        result = (summed / total).astype(BF16)
+        return [result[head * count : (head + 1) * count] for head in range(group)]
+
+    def att_copy(slot, source):
+        return remote(
+            att_send.at[slot], att_recv.at[source], a_s.at[slot], a_r.at[source],
+            {"tp": order[slot]},
+        )
+
+    def place_rows(dst, pieces, start=0, count=rows):
+        for head, piece in enumerate(pieces):
+            dst[pl.ds(start, count), head * HEAD_DIM : (head + 1) * HEAD_DIM] = piece
+
+    returned = []
+    for slot in (3, 2, 1):
+        if slot == 3:
+            for piece, span in enumerate(far_spans):
+                place_rows(att_send.at[slot], ready_rows(far_carried[piece], 3, *span), *span)
+        else:
+            place_rows(att_send.at[slot], ready_rows(carried[slot], slot))
+        copy = att_copy(slot, tp)
+        copy.start()
+        sent.append(copy)
+        returned.append(att_copy(slot, order[slot]))
+    place_rows(att_recv.at[tp], ready_rows(carried[0], 0))
+    ready("ogain", "wout")
+    for copy in returned:
+        copy.wait_recv()
+
+    tokens = jnp.concatenate([att_recv[place] for place in range(n_tp)], 1).astype(F32)
+    inverse = lax.rsqrt(jnp.mean(tokens * tokens, -1, keepdims=True) + EPSILON)
+    att_normed = (tokens * inverse * ogain_v[...]).astype(BF16)
+    wide = width // 2
+    for place in range(2):
+        columns = slice(place * wide, (place + 1) * wide)
+        mixture = jnp.dot(att_normed, wout_v[:, columns], preferred_element_type=F32)
+        out_ref[0, :, columns] = (
+            x_all[0, :, columns].astype(F32) + gate[:, columns] * mixture
+        ).astype(BF16)
+    sent.extend(shared.values())
+    for copy in sent:
+        copy.wait_send()
+
+    @pl.when(hub)
+    def _():
+        for make, given in hub_sent:
+            make(*given).wait_send()
+
+    @pl.when(edge)
+    def _():
+        for make, given in edge_sent:
+            make(*given).wait_send()
+
+
+def line_call(operands):
+    latent, context, w_shift, w_query, w_out = (operands[i] for i in (0, 2, 4, 8, 15))
+    n_sp, n_tp, planes = 2, 4, 8
+    rows, width = latent.shape[1:]
+    ctx_rows = context.shape[1]
+    in_rows, mod_cols = w_shift.shape
+    q_cols = w_query.shape[1]
+    group = q_cols // HEAD_DIM
+    inner = w_out.shape[0]
+    qkv_cols = q_cols + 2 * HEAD_DIM
+    assert rows % (16 * PARTS) == 0 and width % (planes * SHARD_PIECES * 16) == 0
+    dma = pltpu.SemaphoreType.DMA
+    return pl.pallas_call(
+        line_kernel,
+        out_shape=pltpu.VMEM(latent.shape, BF16),
+        in_specs=[pl.BlockSpec(memory_space=pl.ANY)] * len(operands),
+        out_specs=pl.BlockSpec(memory_space=pltpu.VMEM),
+        scratch_shapes=[
+            pltpu.VMEM((n_tp, rows, width), BF16),
+            pltpu.VMEM((1, width), BF16),
+            pltpu.VMEM((width,), BF16),
+            pltpu.VMEM((ctx_rows, width), BF16),
+            pltpu.VMEM((3, in_rows, mod_cols), BF16),
+            pltpu.VMEM((1, width), F32),
+            pltpu.VMEM((width, qkv_cols), BF16),
+            pltpu.VMEM((width, qkv_cols), BF16),
+            pltpu.VMEM((width // planes, qkv_cols), BF16),
+            pltpu.VMEM((1, HEAD_DIM), F32),
+            pltpu.VMEM((1, HEAD_DIM), F32),
+            pltpu.VMEM((1, group), F32),
+            pltpu.VMEM((1, inner), F32),
+            pltpu.VMEM((inner, width), BF16),
+            pltpu.VMEM((2, n_tp * rows, HEAD_DIM), F32),
+            pltpu.VMEM((8, mod_cols), F32),
+            pltpu.VMEM((8, mod_cols), F32),
+            pltpu.VMEM((8, mod_cols), F32),
+            pltpu.VMEM((n_tp, 8, mod_cols), F32),
+            pltpu.VMEM((n_sp, n_tp, rows, 2 * HEAD_DIM), BF16),
+            pltpu.VMEM((n_sp, ctx_rows, 2 * HEAD_DIM), BF16),
+            pltpu.VMEM((n_tp, group, rows, HEAD_DIM), BF16),
+            pltpu.VMEM((group, rows, HEAD_DIM), BF16),
+            pltpu.VMEM((rows, 2 * HEAD_DIM), BF16),
+            pltpu.VMEM((n_tp, rows, q_cols), BF16),
+            pltpu.VMEM((n_tp, rows, q_cols), BF16),
+            pltpu.VMEM((1, width), F32),
+            dma((len(operands) + 3,)),
+            pltpu.SemaphoreType.REGULAR,
+            dma((2, PARTS)),
+            dma((2, PARTS)),
+            dma((3, PARTS)),
+            dma, dma,
+            dma((n_tp,)),
+            dma((n_tp,)),
+            dma((6,)),
+            dma((6,)),
+            dma((n_tp,)),
+            dma((n_tp,)),
+            dma((SHARD_PIECES,)),
+            dma((SHARD_PIECES,)),
+            dma((SHARD_PIECES + 2,)),
+            dma((SHARD_PIECES + 2,)),
+            dma((SHARD_PIECES + 2,)),
+            dma((SHARD_PIECES + 2,)),
+            dma((4, SHARD_PIECES)),
+            dma((4, SHARD_PIECES)),
+            dma((2,)),
+            dma((2,)),
+            dma((2, n_sp)),
+            dma((2, n_sp)),
+        ],
+        compiler_params=pltpu.CompilerParams(
+            collective_id=0, has_side_effects=True, vmem_limit_bytes=60 * 2**20
+        ),
+    )(*operands)
+
+
 def solution(mesh):
     n_sp, n_tp = mesh.shape["sp"], mesh.shape["tp"]
+    planes = (mesh.shape["grp"], n_sp, mesh.shape["dp"])
+    on_line = planes == (2, 2, 2) and n_tp == 4
 
     def on_device(latent, cond, context, cond_ctx, w_shift, w_scale, w_gate, norm_gain, w_query,
                   w_key, w_value, query_gain, key_gain, ctx_lift, out_gain, w_out):
@@ -395,8 +1027,10 @@
             out_gain[None], w_out, table,
         )
         dma = pltpu.SemaphoreType.DMA
+        if on_line:
+            return line_call(operands)
         return pl.pallas_call(
-            functools.partial(kernel, n_sp, n_tp),
+            functools.partial(ring_kernel, n_sp, n_tp),
             out_shape=pltpu.VMEM(latent.shape, BF16),
             in_specs=[pl.BlockSpec(memory_space=pl.ANY)] * len(operands),
             out_specs=pl.BlockSpec(memory_space=pltpu.VMEM),

time: 46.5 us -> 41.5 us (0.89)
  Pallas kernels: 45.6 us -> 40.6 us
    pallas_call x1, Pallas kernels: 45.6 us -> 40.6 us  [line_call(): pl.pallas_call(line_kernel, out_shape=pltpu.VMEM(latent.shape, BF16), in_...]
where the time goes in v1:
time: 41.5 us; the launch traced here: 41.4 us
  Pallas kernels  40.6 us (98%)
  local copies, waits for them, and re-layouts  0.75 us (2%)
    pallas_call x1, Pallas kernels, line_call(): pl.pallas_call(line_kernel, out_shape=pltpu.VMEM(latent.shape, BF16), in_...  40.6 us

profile of v1, /device:TPU:0, one launch (start us, length us, event | category | flops | bytes accessed | tf_op | source)
XLA Modules:
  0.0 41.4 jit_solution(14837649440048809933)
XLA Ops:
  0.0 40.6 %shard_map.163 = bf16[1,96,2048]{2,1,0:T(8,128)(2,1)S(1)} custom-call(bf16[1,96,2048]{2,1,0:T(8,128)(2,1)} %refs_0_.1, bf16[1,2048]{1,0:T(2,128)(2,1)} %refs_1_.1, bf16[1,128,2048]{2,1,0:T(8,128)(2,1)} %refs_2_.1, bf16[2048]{0:T(1024)(128)(2,1)} %refs_3_.1, bf16[1024,512]{1,0:T(8,128)(2,1)} %refs_4_.1, bf16[1024,512]{1,0:T(8,128)(2,1)} %refs_5_.1, ...), custom_call_target="tpu_custom_call" | custom-call | tf_op jit(solution)/shard_map/pallas_call | solution.py:944
  40.7 0.7 %copy.19 = bf16[1,96,2048]{2,1,0:T(8,128)(2,1)} copy(bf16[1,96,2048]{2,1,0:T(8,128)(2,1)S(1)} %shard_map.163) | data formatting | bytes 786432
